TPU v7x, 32 devices: a whole 2x2x4 slice. The times are simulated.
32 devices in a mesh: kv: 16 (over z, y, x), tp: 2 (over core).
Axes of the slice: x: 2, y: 2, z: 4, core: 2. Of those that a mesh axis runs over, the one named last changes fastest.
Arguments:
- tokens: bfloat16 [32, 4096], P(None, 'kv'), may hold values from -12 to 12
- norm_gain: float32 [4096], P('kv'), may hold values from 0.1 to 1.9
- query_weight: bfloat16 [4096, 1024], P('kv', 'tp'), may hold values from -0.09375 to 0.09375
- key_weight: bfloat16 [4096, 1024], P('kv', 'tp'), may hold values from -0.09375 to 0.09375
- value_weight: bfloat16 [4096, 1024], P('kv', 'tp'), may hold values from -0.09375 to 0.09375
- forget_weight: bfloat16 [4096, 16], replicated, may hold values from -0.09375 to 0.09375
- forget_bias: float32 [16], replicated, may hold values from -4 to 4
- cache_keys: bfloat16 [32, 4096, 1024], P(None, 'kv', 'tp'), may hold values from -300 to 300
- cache_values: bfloat16 [32, 4096, 1024], P(None, 'kv', 'tp'), may hold values from -6 to 6
- cum_gate: float32 [32, 16, 4096], P(None, 'tp', 'kv'), may hold values from -4096 to 0, as said below
- lengths: int32 [32], replicated, may hold values from 1 to 4096, as said below
- out_weight: bfloat16 [1024, 4096], P('tp', 'kv'), may hold values from -0.75 to 0.75
- mlp_gain: float32 [4096], P('kv'), may hold values from 0.1 to 1.9
- up_weight: bfloat16 [4096, 16384], P('kv', 'tp'), may hold values from -0.09375 to 0.09375
- down_weight: bfloat16 [16384, 4096], P('tp', 'kv'), may hold values from -0.046875 to 0.046875
Outputs:
- layer_out: bfloat16 [32, 4096], P(None, 'kv')
Inputs may be any that keep to these rules, and one draw needn't show every extreme that they name: The first lengths[b] cache positions of sequence b are live; some sequence has all 4096 positions live. `cum_gate`: never falls from one position to the next, and is 0 from position lengths[b] - 1 on.
All inputs are finite; a program needn't handle non-finite values.
Results may differ from a plain program's by a relative error of at most 0.017.
Values may be sent and summed in bfloat16 or wider, within the bound.
A program may use at most 128 MiB of HBM per device.

v0:
```python
import jax
import jax.numpy as jnp
from jax import lax
from jax.sharding import PartitionSpec as P

HEAD = 64


EPSILON = 1e-06


def joined(part, axis, combine):
    gathered = jax.tree.map(lambda a: lax.all_gather(a, axis), part)

    def take(source):
        return jax.tree.map(lambda a: lax.dynamic_index_in_dim(a, source, 0, False), gathered)

    return lax.fori_loop(
        1, lax.axis_size(axis), lambda source, state: combine(state, take(source)), take(0)
    )


def weighted_merge(first, second):
    peak_a, total_a, accum_a = first
    peak_b, total_b, accum_b = second
    peak = jnp.maximum(peak_a, peak_b)
    factor_a = jnp.exp(peak_a - peak)
    factor_b = jnp.exp(peak_b - peak)
    accum = accum_a * jnp.repeat(factor_a, HEAD, axis=1) + accum_b * jnp.repeat(
        factor_b, HEAD, axis=1
    )
    return (peak, total_a * factor_a + total_b * factor_b, accum)


def shards(
    tokens,
    norm_gain,
    query_weight,
    key_weight,
    value_weight,
    forget_weight,
    forget_bias,
    cache_keys,
    cache_values,
    cum_gate,
    lengths,
    out_weight,
    mlp_gain,
    up_weight,
    down_weight,
):
    kv_rank = lax.axis_index("kv")
    tp_rank = lax.axis_index("tp")
    kv_count = lax.axis_size("kv")
    seqs_here, own_cols = tokens.shape
    model_width = own_cols * kv_count
    head_cols = query_weight.shape[1]
    heads_here = head_cols // HEAD
    span = cache_keys.shape[1]
    scale = HEAD ** (-0.5)
    tok_float = tokens.astype(jnp.float32)
    normed = (tok_float * norm_gain).astype(jnp.bfloat16)
    forget_rows = lax.dynamic_slice_in_dim(forget_weight, kv_rank * own_cols, own_cols, 0)
    squares, query_sum, key_sum, value_sum, forget_sum = lax.psum(
        (
            jnp.sum(tok_float * tok_float, axis=1),
            jnp.dot(normed, query_weight, preferred_element_type=jnp.float32),
            jnp.dot(normed, key_weight, preferred_element_type=jnp.float32),
            jnp.dot(normed, value_weight, preferred_element_type=jnp.float32),
            jnp.dot(normed, forget_rows, preferred_element_type=jnp.float32),
        ),
        "kv",
    )
    inv_rms = lax.rsqrt(squares / model_width + EPSILON)[:, None]
    query = (inv_rms * query_sum).astype(jnp.bfloat16)
    new_key = (inv_rms * key_sum).astype(jnp.bfloat16)
    new_value = (inv_rms * value_sum).astype(jnp.bfloat16)
    forget_all = jax.nn.log_sigmoid(inv_rms * forget_sum + forget_bias)
    forget_here = lax.dynamic_slice_in_dim(forget_all, tp_rank * heads_here, heads_here, 1)
    query_heads = query.reshape(seqs_here, heads_here, HEAD)
    key_heads = cache_keys.reshape(seqs_here, span, heads_here, HEAD)
    value_heads = cache_values.reshape(seqs_here, span, heads_here, HEAD)
    scores = (
        jnp.einsum("bhd,bphd->bhp", query_heads, key_heads, preferred_element_type=jnp.float32)
        * scale
    )
    scores = scores + cum_gate + forget_here[:, :, None]
    positions = kv_rank * span + lax.iota(jnp.int32, span)
    live = positions[None, None, :] < lengths[:, None, None]
    scores = jnp.where(live, scores, -1e30)
    peak = jnp.max(scores, axis=2)
    weights = jnp.where(live, jnp.exp(scores - peak[:, :, None]), 0.0)
    total = jnp.sum(weights, axis=2)
    accum = jnp.einsum(
        "bhp,bphd->bhd",
        weights.astype(jnp.bfloat16),
        value_heads,
        preferred_element_type=jnp.float32,
    ).reshape(seqs_here, head_cols)
    peak, total, accum = joined((peak, total, accum), "kv", weighted_merge)
    own_score = (
        jnp.sum(
            query_heads.astype(jnp.float32)
            * new_key.reshape(seqs_here, heads_here, HEAD).astype(jnp.float32),
            axis=2,
        )
        * scale
    )
    top = jnp.maximum(peak, own_score)
    cache_factor = jnp.exp(peak - top)
    own_weight = jnp.exp(own_score - top)
    denom = total * cache_factor + own_weight
    own_rounded = own_weight.astype(jnp.bfloat16).astype(jnp.float32)
    numer = accum.reshape(seqs_here, heads_here, HEAD) * cache_factor[:, :, None]
    numer = numer + own_rounded[:, :, None] * new_value.reshape(seqs_here, heads_here, HEAD).astype(
        jnp.float32
    )
    attended = (numer / denom[:, :, None]).reshape(seqs_here, head_cols).astype(jnp.bfloat16)
    mixed = lax.psum(
        jnp.dot(attended, out_weight, preferred_element_type=jnp.float32).astype(jnp.bfloat16), "tp"
    ).astype(jnp.float32)
    hidden_in = (tok_float + mixed).astype(jnp.bfloat16)
    hidden_float = hidden_in.astype(jnp.float32)
    mlp_in = (hidden_float * mlp_gain).astype(jnp.bfloat16)
    up_part = jnp.dot(mlp_in, up_weight, preferred_element_type=jnp.float32)
    hidden_squares = jnp.sum(hidden_float * hidden_float, axis=1)
    second_sq, up_total = lax.psum((hidden_squares, up_part), "kv")
    second_rms = lax.rsqrt(second_sq / model_width + EPSILON)[:, None]
    activated = jnp.square(jax.nn.relu(second_rms * up_total)).astype(jnp.bfloat16)
    down_part = jnp.dot(activated, down_weight, preferred_element_type=jnp.float32)
    down_total = lax.psum(down_part.astype(jnp.bfloat16), "tp").astype(jnp.float32)
    return (hidden_float + down_total).astype(jnp.bfloat16)


def solution(mesh):
    return jax.shard_map(
        shards,
        mesh=mesh,
        in_specs=(
            P(None, "kv"),
            P("kv"),
            P("kv", "tp"),
            P("kv", "tp"),
            P("kv", "tp"),
            P(),
            P(),
            P(None, "kv", "tp"),
            P(None, "kv", "tp"),
            P(None, "tp", "kv"),
            P(),
            P("tp", "kv"),
            P("kv"),
            P("kv", "tp"),
            P("tp", "kv"),
        ),
        out_specs=P(None, "kv"),
        check_vma=False,
    )
```

profile of v0, /device:TPU:29, one launch (start us, length us, event | category | flops | bytes accessed | tf_op | source)
XLA Modules:
  0.0 363.1 jit_solution(11094373273417405335)
XLA Ops:
  6.5 0.9 copy-done
  7.5 1.5 fusion.30
  9.0 1.7 fusion.26
  10.7 1.8 fusion.24
  12.6 0.8 fusion.13
  13.4 0.9 fusion.28
  14.3 29.6 %all-reduce = (f32[32]{0:T(128)S(1)}, f32[32,16]{0,1:T(8,128)S(1)}) all-reduce(f32[32]{0:T(128)S(1)} %fusion.13, f32[32,16]{0,1:T(8,128)S(1)} %fusion.28), channel_id=1, replica_groups=mesh['kv'=16,'tp'=2] {'kv'}, use_global_device_ids=true, to_apply=%region_1.0 | all-reduce | flops 544 | bytes 4352 | tf_op jit(solution)/shard_map/psum | solution.py:64
  43.9 0.7 fusion.45
  44.7 11.9 %copy.44 = bf16[32,256,512]{1,2,0:T(8,128)(2,1)} copy(bf16[32,256,512]{2,1,0:T(8,128)(2,1)} %param.24) | data formatting | bytes 16777216 | tf_op args[7]
  56.7 11.9 %copy.48 = bf16[32,256,512]{1,2,0:T(8,128)(2,1)} copy(bf16[32,256,512]{2,1,0:T(8,128)(2,1)} %param.25) | data formatting | bytes 16777216 | tf_op args[8]
  68.6 51.5 %all-reduce.7.cloned.1.call-done = (f32[32,512]{1,0:T(8,128)}, f32[32,512]{1,0:T(8,128)}, f32[32,512]{1,0:T(8,128)}) async-done(((f32[32,512]{1,0:T(8,128)}, f32[32,512]{1,0:T(8,128)}, f32[32,512]{1,0:T(8,128)}), (f32[32,512]{1,0:T(8,128)}, f32[32,512]{1,0:T(8,128)}, f32[32,512]{1,0:T(8,128)})) %all-reduce.7.cloned.1.call-update) | async-done | bytes 196624 | tf_op jit(solution)/shard_map/psum | solution.py:64
  120.1 0.9 fusion.19
  121.1 0.1 reshape.104
  121.2 4.7 %fusion.46 = f32[32,8,1,256]{3,2,1,0:T(1,128)S(1)} fusion(bf16[32,8,64,1]{2,3,1,0:T(2,128)(2,1)S(1)} %reshape.104, bf16[32,256,8,64]{1,3,2,0:T(8,128)(2,1)} %bitcast.51), kind=kOutput, calls=%fused_computation.73 | convolution fusion | flops 8388608 | bytes 8683520 | tf_op jit(solution)/shard_map/bhd,bphd->bhp/dot_general | solution.py:84
  125.9 0.2 fusion.43
  126.1 0.2 fusion.12
  126.3 0.7 slice-done.1
  127.0 2.3 fusion.8
  129.3 0.7 all_gather_reshape.3
  130.1 0.1 reshape.81
  130.3 0.1 multiply_reduce_fusion
  130.6 26.6 %all-gather.2 = f32[16,32,8]{1,2,0:T(8,128)S(1)} all-gather(f32[1,32,8]{1,2,0:T(8,128)S(1)} %copy.46), channel_id=2, replica_groups=mesh['kv'=16,'tp'=2] {'kv'}, dimensions={0}, use_global_device_ids=true | all-gather | bytes 17408 | tf_op jit(solution)/shard_map/all_gather | solution.py:13
  157.3 31.4 %all-gather.3 = f32[16,32,8]{1,2,0:T(8,128)S(1)} all-gather(f32[1,32,8]{1,2,0:T(8,128)S(1)} %copy.47), channel_id=3, replica_groups=mesh['kv'=16,'tp'=2] {'kv'}, dimensions={0}, use_global_device_ids=true | all-gather | bytes 17408 | tf_op jit(solution)/shard_map/all_gather | solution.py:13
  188.6 0.8 slice_bitcast_fusion
  189.5 21.8 %while.19 = (s32[]{:T(128)}, f32[32,8]{0,1:T(8,128)S(1)}, f32[32,8]{0,1:T(8,128)S(1)}, f32[32,512]{1,0:T(8,128)S(1)}, f32[16,32,8]{1,2,0:T(8,128)S(1)}, /*index=...) while((s32[]{:T(128)}, f32[32,8]{0,1:T(8,128)S(1)}, ...), condition=%wide.region_7.8_spmd, body=%wide.region_6.7_spmd.sunk | while | flops 50693 | bytes 735375 | solution.py:18
  189.7 0.1 reshape.108
  190.0 0.9 fusion.59
  191.2 0.1 reshape.108
  191.4 0.1 reshape.107
  191.5 0.9 fusion.59
  192.6 0.1 reshape.108
  192.8 0.1 reshape.107
  192.9 0.9 fusion.59
  194.1 0.1 reshape.108
  194.3 0.1 reshape.107
  194.4 0.9 fusion.59
  195.5 0.1 reshape.108
  195.7 0.1 reshape.107
  195.8 0.9 fusion.59
  197.0 0.1 reshape.108
  197.3 0.9 fusion.59
  198.7 0.1 reshape.107
  198.8 0.9 fusion.59
  199.9 0.1 reshape.108
  200.1 0.1 reshape.107
  200.2 0.9 fusion.59
  201.4 0.1 reshape.108
  201.6 0.1 reshape.107
  201.7 0.9 fusion.59
  203.1 0.9 fusion.59
  204.6 0.9 fusion.59
  206.0 0.9 fusion.59
  207.5 0.9 fusion.59
  209.0 0.9 fusion.59
  210.4 0.9 fusion.59
  212.1 0.2 convolution_convert_fusion.1
  212.3 19.6 %psum.68 = bf16[32,256]{1,0:T(8,128)(2,1)S(1)} all-reduce(bf16[32,256]{1,0:T(8,128)(2,1)S(1)} %convolution_convert_fusion.1), channel_id=1, replica_groups=mesh['kv'=16,'tp'=2] {'tp'}, use_global_device_ids=true, to_apply=%region_11.12 | all-reduce | flops 8192 | bytes 32768 | tf_op jit(solution)/shard_map/psum | solution.py:119
  232.0 4.1 %fusion.21 = f32[32,8192]{1,0:T(8,128)} fusion(bf16[256,8192]{1,0:T(8,128)(2,1)} %param.30, f32[256]{0:T(256)S(1)} %copy-done.5, bf16[32,256]{1,0:T(8,128)(2,1)S(1)} %copy-done.1, bf16[32,256]{1,0:T(8,128)(2,1)S(1)} %psum.68), kind=kOutput, calls=%fused_computation.43 | convolution fusion | flops 134275072 | bytes 5276672 | tf_op jit(solution)/shard_map/dot_general | solution.py:125
  236.1 0.1 fusion.16
  236.2 30.3 %psum.69 = f32[32]{0:T(128)S(1)} all-reduce(f32[32]{0:T(128)S(1)} %fusion.16), channel_id=1, replica_groups=mesh['kv'=16,'tp'=2] {'kv'}, use_global_device_ids=true, to_apply=%region_13.14 | all-reduce | flops 32 | bytes 256 | tf_op jit(solution)/shard_map/psum | solution.py:127
  266.5 80.1 %all-reduce.5.cloned.1.call-done = f32[32,8192]{1,0:T(8,128)} async-done(((f32[32,8192]{1,0:T(8,128)}), f32[32,8192]{1,0:T(8,128)}) %all-reduce.5.cloned.1.call-update) | async-done | bytes 1048592 | tf_op jit(solution)/shard_map/psum | solution.py:127
  346.6 3.4 convolution_convert_fusion
  350.0 6.0 %psum.71 = bf16[32,256]{1,0:T(8,128)(2,1)S(1)} all-reduce(bf16[32,256]{1,0:T(8,128)(2,1)S(1)} %convolution_convert_fusion), channel_id=1, replica_groups=mesh['kv'=16,'tp'=2] {'tp'}, use_global_device_ids=true, to_apply=%region_15.16 | all-reduce | flops 8192 | bytes 32768 | tf_op jit(solution)/shard_map/psum | solution.py:131
  356.0 0.6 fusion.18
  (136 shorter events, 8.0 us)
Async XLA Ops:
  6.5 1.0 copy-start
  6.5 113.6 %all-reduce.7.cloned.1.call-start = ((), (), s32[]{:S(2)}) async-start(), calls=%async_computation.2 | async-start | bytes 393216 | tf_op jit(solution)/shard_map/psum | solution.py:64
  12.5 176.1 %all-gather.6.cloned.1.call-start = ((), (), s32[]{:S(2)}) async-start(), calls=%async_computation | async-start | bytes 1114112 | tf_op jit(solution)/shard_map/all_gather | solution.py:13
  56.7 11.9 %copy-start.6 = (s32[32]{0:T(128)S(1)}, s32[32]{0:T(128)}, u32[]{:S(2)}) copy-start(s32[32]{0:T(128)} %param.27) | copy-start | bytes 388
  68.6 57.4 %copy-start.2 = (f32[32,8,256]{2,1,0:T(8,128)S(1)}, f32[32,8,256]{2,1,0:T(8,128)}, u32[]{:S(2)}) copy-start(f32[32,8,256]{2,1,0:T(8,128)} %param.26) | copy-start | bytes 786436
  121.2 5.2 %slice-start = ((s8[8388608]{0:T(1024)(128)(4,1)}), s8[4194304]{0:T(1024)(128)(4,1)S(1)}, s32[]{:S(2)}) async-start(s8[8388608]{0:T(1024)(128)(4,1)} %bitcast.52), calls=%async_computation.3 | async-start | bytes 8388608
  121.2 5.8 %slice-start.1 = ((s8[8388608]{0:T(1024)(128)(4,1)}), s8[4194304]{0:T(1024)(128)(4,1)S(1)}, s32[]{:S(2)}) async-start(s8[8388608]{0:T(1024)(128)(4,1)} %bitcast.52), calls=%async_computation.4 | async-start | bytes 8388608
  127.0 85.1 %copy-start.3 = (bf16[512,256]{1,0:T(8,128)(2,1)S(1)}, bf16[512,256]{1,0:T(8,128)(2,1)}, u32[]{:S(2)}) copy-start(bf16[512,256]{1,0:T(8,128)(2,1)} %param.28) | copy-start | bytes 786436
  127.0 85.1 %copy-start.4 = (f32[32,512]{1,0:T(8,128)S(1)}, f32[32,512]{1,0:T(8,128)}, u32[]{:S(2)}) copy-start(f32[32,512]{1,0:T(8,128)} %get-tuple-element.204) | copy-start | bytes 196612
  127.0 104.9 %copy-start.1 = (bf16[32,256]{1,0:T(8,128)(2,1)S(1)}, bf16[32,256]{1,0:T(8,128)(2,1)}, u32[]{:S(2)}) copy-start(bf16[32,256]{1,0:T(8,128)(2,1)} %param.17) | copy-start | bytes 49156
  127.0 104.9 %copy-start.5 = (f32[256]{0:T(256)S(1)}, f32[256]{0:T(256)}, u32[]{:S(2)}) copy-start(f32[256]{0:T(256)} %param.29) | copy-start | bytes 3076
  130.1 216.5 %all-reduce.5.cloned.1.call-start = ((), (), s32[]{:S(2)}) async-start(), calls=%async_computation.1 | async-start | bytes 2097152 | tf_op jit(solution)/shard_map/psum | solution.py:127
Sparse Core Ops, SparseCore 0:
  13.0 107.0 all-reduce.6
  130.2 53.8 all-gather.5
  236.2 110.3 all-reduce.4
where the time goes:
time: 368 us; the launch traced here: 363 us
  blocking collectives  144 us (39%)
  waiting for transfers between devices  132 us (36%)
  local copies, waits for them, and re-layouts  36.2 us (10%)
  matrix products  20.5 us (6%)
  other arithmetic  17.2 us (5%)
  between operations  13.3 us (4%)
    psum x1, waiting for transfers between devices, shards(): second_sq, up_total = lax.psum((hidden_squares, up_part), 'kv')  80.1 us
    all_gather x2, blocking collectives, joined(): gathered = jax.tree.map(lambda a: lax.all_gather(a, axis), part)  58 us
    psum x1, waiting for transfers between devices, shards(): lax.psum((jnp.sum(tok_float * tok_float, axis=1), jnp.dot(normed, query_w...  51.5 us
    psum x1, blocking collectives, shards(): second_sq, up_total = lax.psum((hidden_squares, up_part), 'kv')  30.3 us
    psum x1, blocking collectives, shards(): lax.psum((jnp.sum(tok_float * tok_float, axis=1), jnp.dot(normed, query_w...  29.6 us
    unnamed x22, local copies, waits for them, and re-layouts  25.6 us
    psum x1, blocking collectives, shards(): lax.psum(jnp.dot(attended, out_weight, preferred_element_type=jnp.float32...  19.6 us
    add x15, other arithmetic, weighted_merge(): accum_a * jnp.repeat(factor_a, HEAD, axis=1)  13.1 us
  transfers between devices with their start and end apart: 3, of which 2 were waited for; matrix products, arithmetic and copies ran while one was open for 7% of the time, Pallas kernels for 0%

commit v1 on v0

--- a/solution.py
+++ b/solution.py
@@ -1,6 +1,10 @@
+import functools
+
 import jax
 import jax.numpy as jnp
 from jax import lax
+from jax.experimental import pallas as pl
+from jax.experimental.pallas import tpu as pltpu
 from jax.sharding import PartitionSpec as P
 
 HEAD = 64
@@ -132,9 +136,378 @@
     return (hidden_float + down_total).astype(jnp.bfloat16)
 
 
+LANES = 128
+NEG = -1e30
+MESH = pl.DeviceIdType.MESH
+F32 = jnp.float32
+BF16 = jnp.bfloat16
+QKV_SUM, QUERY_ALL, CACHE_SUM, ATT_ALL, MIX_PAIR, UP_SUM, SQ_ALL, ACT_ALL, DOWN_PAIR = range(9)
+
+
+def lane_pick(x, lane, index):
+    return jnp.sum(jnp.where(lane == index, x, 0.0), axis=-1, keepdims=True)
+
+
+def step_kernel(n, nt, dims, *refs):
+    rows, cols, heads, span, hidden, width = dims
+    own = rows // n
+    head_cols = heads * HEAD
+    chunk = hidden // n
+    len_ref = refs[0]
+    sources = refs[1:15]
+    out_ref = refs[15]
+    held = refs[16:30]
+    (extra, a_send, a_recv, q_own, q_all, c_send, c_recv, t_own, t_all, att, x_own, x_all,
+     d_send, d_recv, s_own, s_all, g_own, g_all, y_own, y_all,
+     lsem, ssem, rsem, psend, precv) = refs[30:]
+    tok, ng, wq, wk, wv, fw, fb, ck, cv, cg, ow, mg, uw, dw = held
+    me = lax.axis_index("kv")
+    tp = lax.axis_index("tp")
+
+    local = []
+    for i, (source, target) in enumerate(zip(sources, held)):
+        if i == 5:
+            source = source.at[pl.ds(pl.multiple_of(me * cols, cols), cols), :]
+        local.append(pltpu.make_async_copy(source, target, lsem.at[i]))
+    for i in range(7):
+        local[i].start()
+
+    barrier = pltpu.get_barrier_semaphore()
+
+    def greet(t, carry):
+        pl.semaphore_signal(
+            barrier, inc=1, device_id={"kv": lax.rem(me + t, n)}, device_id_type=MESH
+        )
+        return carry
+
+    lax.fori_loop(1, n, greet, 0)
+    for t in range(1, nt):
+        pl.semaphore_signal(
+            barrier, inc=1, device_id={"tp": lax.rem(tp + t, nt)}, device_id_type=MESH
+        )
+    for i in (7, 9, 8, 11, 10, 12, 13):
+        local[i].start()
+
+    def remote(phase, source, target, peer, slot):
+        return pltpu.make_async_remote_copy(
+            src_ref=source, dst_ref=target.at[slot], send_sem=ssem.at[phase, peer],
+            recv_sem=rsem.at[phase, slot], device_id={"kv": peer}, device_id_type=MESH,
+        )
+
+    def send_to(phase, source_of, target, t):
+        peer = lax.rem(me + t, n)
+        remote(phase, source_of(peer), target, peer, me).start()
+
+    def send_all(phase, source_of, target):
+        def step(t, carry):
+            send_to(phase, source_of, target, t)
+            return carry
+
+        lax.fori_loop(1, n, step, 0)
+
+    def wait_from(phase, source_of, target, t):
+        peer = lax.rem(me + n - t, n)
+        remote(phase, source_of(peer), target, peer, peer).wait_recv()
+        return peer
+
+    def wait_all(phase, source_of, target):
+        def step(t, carry):
+            wait_from(phase, source_of, target, t)
+            return carry
+
+        lax.fori_loop(1, n, step, 0)
+
+    def sent_all(phase, source_of, target):
+        def step(t, carry):
+            peer = lax.rem(me + t, n)
+            remote(phase, source_of(peer), target, peer, me).wait_send()
+            return carry
+
+        lax.fori_loop(1, n, step, 0)
+
+    def pair(index, source, target, t):
+        peer = lax.rem(tp + t, nt)
+        return pltpu.make_async_remote_copy(
+            src_ref=source, dst_ref=target.at[tp], send_sem=psend.at[index, peer],
+            recv_sem=precv.at[index, tp], device_id={"tp": peer}, device_id_type=MESH,
+        )
+
+    def pair_in(index, source, target, t):
+        peer = lax.rem(tp + t, nt)
+        return pltpu.make_async_remote_copy(
+            src_ref=source, dst_ref=target.at[peer], send_sem=psend.at[index, peer],
+            recv_sem=precv.at[index, peer], device_id={"tp": peer}, device_id_type=MESH,
+        )
+
+    lane = lax.broadcasted_iota(jnp.int32, (heads, LANES), 1)
+    head = lax.broadcasted_iota(jnp.int32, (heads, LANES), 0)
+    wide_lane = lax.broadcasted_iota(jnp.int32, (heads, head_cols), 1)
+    wide_head = lax.broadcasted_iota(jnp.int32, (heads, head_cols), 0)
+    mine = (wide_lane >= wide_head * HEAD) & (wide_lane < (wide_head + 1) * HEAD)
+
+    def fold(x):
+        x = jnp.where(mine, x, 0.0)
+        total = x[:, :LANES]
+        for k in range(1, head_cols // LANES):
+            total = total + x[:, k * LANES:(k + 1) * LANES]
+        return total + pltpu.roll(total, HEAD, axis=1)
+
+    def spread(row):
+        return fold(jnp.broadcast_to(row, (heads, head_cols)))
+
+    def unfold(x):
+        wide = jnp.concatenate([x] * (head_cols // LANES), axis=1)
+        return jnp.sum(jnp.where(mine, wide, 0.0), axis=0, keepdims=True)
+
+    for i in range(7):
+        local[i].wait()
+    tok_float = tok[...].astype(F32)
+    normed = (tok_float * ng[...]).astype(BF16)
+    extra[...] = jnp.zeros_like(extra)
+    n_forget = fw.shape[1]
+    extra[:, :n_forget] = jnp.dot(normed, fw[...], preferred_element_type=F32)
+    extra[:, n_forget:n_forget + 1] = jnp.sum(tok_float * tok_float, axis=1, keepdims=True)
+    for k, (w, at) in enumerate(((wq, 0), (wk, head_cols), (wv, 2 * head_cols), (None, 3 * head_cols))):
+        if w is None:
+            value, size = extra[...], LANES
+        else:
+            value, size = jnp.dot(normed, w[...], preferred_element_type=F32), head_cols
+        for j in range(n):
+            a_send[j, :, at:at + size] = value[j * own:(j + 1) * own, :]
+    a_recv[me] = a_send[me]
+    pl.semaphore_wait(barrier, n - 1 + nt - 1)
+    part = lambda peer: a_send.at[peer]
+    send_all(QKV_SUM, part, a_recv)
+    wait_all(QKV_SUM, part, a_recv)
+    total = jnp.sum(a_recv[...], axis=0)
+    tail_lane = lax.broadcasted_iota(jnp.int32, (own, LANES), 1)
+    tail = total[:, 3 * head_cols:]
+    inv_rms = lax.rsqrt(lane_pick(tail, tail_lane, n_forget) / width + EPSILON)
+    query = (inv_rms * total[:, :head_cols]).astype(BF16).astype(F32) * HEAD ** (-0.5)
+    new_key = (inv_rms * total[:, head_cols:2 * head_cols]).astype(BF16).astype(F32)
+    new_value = (inv_rms * total[:, 2 * head_cols:3 * head_cols]).astype(BF16).astype(F32)
+    gate_in = inv_rms * tail
+    q_own[...] = query
+    q_all[me] = query
+    q_src = lambda peer: q_own
+    send_all(QUERY_ALL, q_src, q_all)
+
+    own_terms = []
+    for r in range(own):
+        qf, kf, vf = (spread(x[r:r + 1, :]) for x in (query, new_key, new_value))
+        score = jnp.sum(qf * kf, axis=1, keepdims=True) * 0.5
+        raw = jnp.broadcast_to(gate_in[r:r + 1, :], (heads, LANES))
+        raw = lane_pick(raw, lane, head + tp * heads)
+        small_lane = lax.broadcasted_iota(jnp.int32, (heads, n_forget), 1)
+        small_head = lax.broadcasted_iota(jnp.int32, (heads, n_forget), 0)
+        bias = lane_pick(
+            jnp.broadcast_to(fb[...], (heads, n_forget)), small_lane, small_head + tp * heads
+        )
+        z = raw + bias
+        forget = jnp.minimum(z, 0.0) - jnp.log1p(jnp.exp(-jnp.abs(z)))
+        own_terms.append((score, forget, vf))
+
+    wait_all(QUERY_ALL, q_src, q_all)
+    for i in (7, 9, 8):
+        local[i].wait()
+    place = me * span + lax.broadcasted_iota(jnp.int32, (heads, span), 1)
+    group = 4 if n % 4 == 0 else 1
+
+    def attend(g, carry):
+        scores = []
+        seqs = [(g * group + u, r) for u in range(group) for r in range(own)]
+        for i, r in seqs:
+            b = i * own + r
+            row = jnp.broadcast_to(q_all[i, r:r + 1, :], (heads, head_cols))
+            blocks = jnp.where(mine, row, 0.0).astype(BF16)
+            s = lax.dot_general(
+                blocks, ck[b], (((1,), (1,)), ((), ())), preferred_element_type=F32
+            )
+            scores.append(jnp.where(place < len_ref[b], s + cg[b], NEG))
+        peaks = [jnp.max(s, axis=1, keepdims=True) for s in scores]
+        weights = [
+            jnp.where(s > 0.1 * NEG, jnp.exp(s - peak), 0.0) for s, peak in zip(scores, peaks)
+        ]
+        totals = [jnp.sum(w, axis=1, keepdims=True) for w in weights]
+        for (i, r), w, peak, tot in zip(seqs, weights, peaks, totals):
+            acc = fold(jnp.dot(w.astype(BF16), cv[i * own + r], preferred_element_type=F32))
+            acc = jnp.where(lane == HEAD, peak, acc)
+            c_send[i, r] = jnp.where(lane == HEAD + 1, tot, acc)
+        return carry
+
+    lax.fori_loop(0, n // group, attend, 0)
+    c_recv[me] = c_send[me]
+    c_src = lambda peer: c_send.at[peer]
+    send_all(CACHE_SUM, c_src, c_recv)
+    wait_all(CACHE_SUM, c_src, c_recv)
+    for r in range(own):
+        score, forget, vf = own_terms[r]
+        parts = c_recv[:, r]
+        peak = lane_pick(parts, lane[None], HEAD) + forget[None]
+        top = jnp.maximum(jnp.max(peak, axis=0), score)
+        merged = jnp.sum(parts * jnp.exp(peak - top[None]), axis=0)
+        own_weight = jnp.exp(score - top)
+        denom = lane_pick(merged, lane, HEAD + 1) + own_weight
+        numer = merged + own_weight.astype(BF16).astype(F32) * vf
+        done = jnp.where(lane < HEAD, numer / denom, 0.0).astype(BF16).astype(F32)
+        t_own[r:r + 1, :] = unfold(done + pltpu.roll(done, HEAD, axis=1))
+    t_all[me] = t_own[...]
+    t_src = lambda peer: t_own
+    send_all(ATT_ALL, t_src, t_all)
+    wait_all(ATT_ALL, t_src, t_all)
+    for j in range(n):
+        att[j * own:(j + 1) * own, :] = t_all[j]
+    for i in (10, 11, 12, 13):
+        local[i].wait()
+    mixed = jnp.dot(att[...].astype(BF16), ow[...], preferred_element_type=F32).astype(BF16)
+    x_own[...] = mixed
+    x_all[tp] = mixed
+    for t in range(1, nt):
+        pair(0, x_own, x_all, t).start()
+    for t in range(1, nt):
+        pair_in(0, x_own, x_all, t).wait_recv()
+    hidden_in = (tok_float + jnp.sum(x_all[...].astype(F32), axis=0)).astype(BF16)
+    hidden_float = hidden_in.astype(F32)
+    mlp_in = (hidden_float * mg[...]).astype(BF16)
+
+    sq_lane = lax.broadcasted_iota(jnp.int32, (rows, LANES), 1)
+    sq_row = lax.broadcasted_iota(jnp.int32, (rows, LANES), 0)
+    squares = jnp.sum(hidden_float * hidden_float, axis=1, keepdims=True)
+    squares = jnp.sum(jnp.where(sq_lane == sq_row, squares, 0.0), axis=0, keepdims=True)
+    s_own[...] = squares
+    s_all[me] = squares
+    s_src = lambda peer: s_own
+    send_all(SQ_ALL, s_src, s_all)
+    d_src = lambda peer: d_send.at[peer]
+
+    def up(j):
+        w = uw[:, pl.ds(pl.multiple_of(j * chunk, chunk), chunk)]
+        return jnp.dot(mlp_in, w, preferred_element_type=F32)
+
+    def up_step(t, carry):
+        peer = lax.rem(me + t, n)
+        d_send[peer] = up(peer).astype(BF16)
+        send_to(UP_SUM, d_src, d_recv, t)
+        return carry
+
+    lax.fori_loop(1, n, up_step, 0)
+    own_up = up(me)
+    wait_all(SQ_ALL, s_src, s_all)
+    second = jnp.broadcast_to(jnp.sum(s_all[...], axis=0), (rows, LANES))
+    second_rms = lax.rsqrt(lane_pick(second, sq_lane, sq_row) / width + EPSILON)
+
+    def up_take(t, acc):
+        peer = wait_from(UP_SUM, d_src, d_recv, t)
+        return acc + d_recv[peer].astype(F32)
+
+    up_total = lax.fori_loop(1, n, up_take, own_up)
+    activated = jnp.square(jnp.maximum(second_rms * up_total, 0.0)).astype(BF16)
+    g_own[...] = activated
+    g_src = lambda peer: g_own
+    send_all(ACT_ALL, g_src, g_all)
+
+    def down(value, j):
+        w = dw[pl.ds(pl.multiple_of(j * chunk, chunk), chunk), :]
+        return jnp.dot(value, w, preferred_element_type=F32)
+
+    def down_step(t, acc):
+        peer = wait_from(ACT_ALL, g_src, g_all, t)
+        return acc + down(g_all[peer], peer)
+
+    part_out = lax.fori_loop(1, n, down_step, down(activated, me)).astype(BF16)
+    y_own[...] = part_out
+    y_all[tp] = part_out
+    for t in range(1, nt):
+        pair(1, y_own, y_all, t).start()
+    for t in range(1, nt):
+        pair_in(1, y_own, y_all, t).wait_recv()
+    out_ref[...] = (hidden_float + jnp.sum(y_all[...].astype(F32), axis=0)).astype(BF16)
+
+    for phase, source_of, target in (
+        (QKV_SUM, part, a_recv), (QUERY_ALL, q_src, q_all), (CACHE_SUM, c_src, c_recv),
+        (ATT_ALL, t_src, t_all), (SQ_ALL, s_src, s_all), (UP_SUM, d_src, d_recv),
+        (ACT_ALL, g_src, g_all),
+    ):
+        sent_all(phase, source_of, target)
+    for t in range(1, nt):
+        pair(0, x_own, x_all, t).wait_send()
+        pair(1, y_own, y_all, t).wait_send()
+
+
+def fits(n, rows, cols, heads, span, hidden):
+    return (
+        rows % n == 0 and rows <= LANES and cols % LANES == 0 and heads == 8
+        and (heads * HEAD) % LANES == 0 and span % LANES == 0 and hidden % (n * LANES) == 0
+    )
+
+
+def fused(tokens, norm_gain, query_weight, key_weight, value_weight, forget_weight, forget_bias,
+          cache_keys, cache_values, cum_gate, lengths, out_weight, mlp_gain, up_weight, down_weight):
+    n, nt = lax.axis_size("kv"), lax.axis_size("tp")
+    rows, cols = tokens.shape
+    heads, span = cum_gate.shape[1:]
+    hidden = up_weight.shape[1]
+    head_cols = heads * HEAD
+    own, chunk = rows // n, hidden // n
+    ops = [
+        tokens, norm_gain[None], query_weight, key_weight, value_weight, forget_weight,
+        forget_bias[None], cache_keys, cache_values, cum_gate, out_weight, mlp_gain[None],
+        up_weight, down_weight,
+    ]
+    shapes = [op.shape for op in ops]
+    shapes[5] = (cols, forget_weight.shape[1])
+    vm = pltpu.VMEM
+    scratch = [vm(shape, op.dtype) for shape, op in zip(shapes, ops)] + [
+        vm((rows, LANES), F32),
+        vm((n, own, 3 * head_cols + LANES), F32),
+        vm((n, own, 3 * head_cols + LANES), F32),
+        vm((own, head_cols), F32),
+        vm((n, own, head_cols), F32),
+        vm((n, own, heads, LANES), F32),
+        vm((n, own, heads, LANES), F32),
+        vm((own, head_cols), F32),
+        vm((n, own, head_cols), F32),
+        vm((rows, head_cols), F32),
+        vm((rows, cols), BF16),
+        vm((nt, rows, cols), BF16),
+        vm((n, rows, chunk), BF16),
+        vm((n, rows, chunk), BF16),
+        vm((1, LANES), F32),
+        vm((n, 1, LANES), F32),
+        vm((rows, chunk), BF16),
+        vm((n, rows, chunk), BF16),
+        vm((rows, cols), BF16),
+        vm((nt, rows, cols), BF16),
+        pltpu.SemaphoreType.DMA((len(ops),)),
+        pltpu.SemaphoreType.DMA((9, n)),
+        pltpu.SemaphoreType.DMA((9, n)),
+        pltpu.SemaphoreType.DMA((2, nt)),
+        pltpu.SemaphoreType.DMA((2, nt)),
+    ]
+    return pl.pallas_call(
+        functools.partial(step_kernel, n, nt, (rows, cols, heads, span, hidden, cols * n)),
+        out_shape=jax.ShapeDtypeStruct((rows, cols), BF16),
+        in_specs=[pl.BlockSpec(memory_space=pltpu.SMEM)]
+        + [pl.BlockSpec(memory_space=pl.ANY)] * len(ops),
+        out_specs=pl.BlockSpec(memory_space=pltpu.VMEM),
+        scratch_shapes=scratch,
+        compiler_params=pltpu.CompilerParams(
+            collective_id=0, has_side_effects=True, vmem_limit_bytes=60 * 1024 * 1024
+        ),
+    )(lengths, *ops)
+
+
+def layer(*args):
+    tokens, cum_gate, up_weight = args[0], args[9], args[13]
+    heads, span = cum_gate.shape[1:]
+    if fits(lax.axis_size("kv"), *tokens.shape, heads, span, up_weight.shape[1]):
+        return fused(*args)
+    return shards(*args)
+
+
 def solution(mesh):
     return jax.shard_map(
-        shards,
+        layer,
         mesh=mesh,
         in_specs=(
             P(None, "kv"),

time: 368 us -> 71.2 us (0.19); the launches traced: 363 us -> 70.9 us
  blocking collectives: 144 us -> 0 us
  waiting for transfers between devices: 132 us -> 0 us
  Pallas kernels: 0 us -> 67.3 us
  local copies, waits for them, and re-layouts: 36.2 us -> 3.56 us
  matrix products: 20.5 us -> 0 us
  other arithmetic: 17.2 us -> 0 us
  between operations: 13.3 us -> 0.01 us
    psum x2 -> x0, waiting for transfers between devices: 132 us -> none  [the longest x1 80.1 us: shards(): second_sq, up_total = lax.psum((hidden_squares, up_part), 'kv')]
    psum x4 -> x0, blocking collectives: 85.5 us -> none  [the longest x1 30.3 us: shards(): second_sq, up_total = lax.psum((hidden_squares, up_part), 'kv')]
    pallas_call x0 -> x1, Pallas kernels: none -> 67.3 us  [fused(): pl.pallas_call(functools.partial(step_kernel, n, nt, (rows, cols, heads,...]
    all_gather x2 -> x0, blocking collectives: 58 us -> none  [joined(): gathered = jax.tree.map(lambda a: lax.all_gather(a, axis), part)]
    unnamed x22 -> x2, local copies, waits for them, and re-layouts: 25.6 us -> 3.56 us
    dot_general x9 -> x0, matrix products: 20.5 us -> none  [the longest x1 4.72 us: shards(): jnp.einsum('bhd,bphd->bhp', query_heads, key_heads, preferred_element_typ...]
    add x31 -> x0, other arithmetic: 13.4 us -> none  [the longest x15 13.1 us: weighted_merge(): accum_a * jnp.repeat(factor_a, HEAD, axis=1)]
  transfers between devices with their start and end apart: 3 -> 0, of which waited for: 2 -> 0; matrix products, arithmetic and copies ran while one was open for 7% -> 0% of each run, Pallas kernels for 0% -> 0%
where the time goes in v1:
time: 71.2 us; the launch traced here: 70.9 us
  Pallas kernels  67.3 us (95%)
  local copies, waits for them, and re-layouts  3.56 us (5%)
    pallas_call x1, Pallas kernels, fused(): pl.pallas_call(functools.partial(step_kernel, n, nt, (rows, cols, heads,...  67.3 us
    unnamed x2, local copies, waits for them, and re-layouts  3.56 us

profile of v1, /device:TPU:29, one launch (start us, length us, event | category | flops | bytes accessed | tf_op | source)
XLA Modules:
  0.0 70.9 jit_solution(6777876956429911583)
XLA Ops:
  0.0 2.2 %copy.16.refs_6_ = bf16[4096,16]{1,0:T(8,128)(2,1)} copy(bf16[4096,16]{0,1:T(8,128)(2,1)} %param.20) | data formatting | bytes 262144 | tf_op args[5]
  2.2 67.3 %shard_map.145 = bf16[32,256]{1,0:T(8,128)(2,1)} custom-call(s32[32]{0:T(128)} %refs_0_.1, bf16[32,256]{1,0:T(8,128)(2,1)} %refs_1_.1, f32[1,256]{1,0:T(1,128)} %bitcast.3, bf16[256,512]{1,0:T(8,128)(2,1)} %refs_3_.1, bf16[256,512]{1,0:T(8,128)(2,1)} %refs_4_.1, bf16[256,512]{1,0:T(8,128)(2,1)} %refs_5_.1, bf16[4096,16]{1,0:T(8,128)(2,1)} %copy.16.refs_6_, ...), custom_call_target="tpu_custom_call" | custom-call | tf_op jit(solution)/shard_map/pallas_call | solution.py:487
  69.5 1.3 %copy.18 = bf16[32,256]{1,0:T(8,128)(2,1)} copy(bf16[32,256]{1,0:T(8,128)(2,1)} %shard_map.145) | data formatting | bytes 32768
